TPU v7x, 32 devices: a whole 2x2x4 slice. The times are simulated.
32 devices in a mesh: grp: 2 (over y), ra: 4 (over z), cb: 4 (over x, core).
Axes of the slice: x: 2, y: 2, z: 4, core: 2. Of those that a mesh axis runs over, the one named last changes fastest.
Arguments:
- tokens: bfloat16 [512, 4096], P('grp', 'cb'), parts along dimension 0, may hold values from -50 to 50
- norm_gains: float32 [3, 4096], P(None, 'cb'), may hold values from 0.1 to 1.9
- gate_weight: float32 [2, 4096, 11264], P(None, 'cb', 'ra'), may hold values from -0.09375 to 0.09375
- value_weight: float32 [2, 4096, 11264], P(None, 'cb', 'ra'), may hold values from -0.09375 to 0.09375
- gate_scale: float32 [2, 11264], P(None, 'ra'), may hold values from 0.3 to 3
- value_scale: float32 [2, 11264], P(None, 'ra'), may hold values from 0.3 to 3
- conv_gate: float32 [2, 3, 11264], P(None, None, 'ra'), may hold values from -3 to 3
- conv_value: float32 [2, 3, 11264], P(None, None, 'ra'), may hold values from -3 to 3
- down_weight: float32 [2, 11264, 4096], P(None, 'ra', 'cb'), may hold values from -0.07537784 to 0.07537784
- down_scale: float32 [2, 4096], P(None, 'cb'), may hold values from 0.3 to 3
Outputs:
- normed_out: bfloat16 [512, 4096], P('grp', 'cb'), parts along dimension 0
There are 2 independent parts, one for each index of `grp`. A program takes and returns all parts, laid end to end along the dimension named above; an argument that names none is the same for every part. Nothing has to cross between parts.
All inputs are finite; a program needn't handle non-finite values.
Results may differ from a plain program's by a relative error of at most 0.012.
The roundings to bfloat16 on the way count: a program that leaves them out, or rounds other values in their place, can miss the bound.
Values may be sent and summed in bfloat16 or wider, within the bound.
A program may use at most 192 MiB of HBM per device.

v0:
```python
import functools

import jax
import jax.numpy as jnp
from jax import lax
from jax.experimental import pallas as pl
from jax.experimental.pallas import tpu as pltpu
from jax.sharding import PartitionSpec as P

epsilon = 1e-06
residual_weight = 0.5


def causal_taps(projected, tap_weights):
    tap_count = tap_weights.shape[0]
    row_count = projected.shape[0]
    padded = jnp.pad(projected, ((tap_count - 1, 0), (0, 0)))
    result = jnp.zeros_like(projected)
    for tap_idx in range(tap_count):
        result = result + padded[tap_idx : tap_idx + row_count] * tap_weights[tap_idx]
    return result


def row_inverse(state_wide, model_width):
    squares = lax.psum(jnp.sum(state_wide * state_wide, axis=1, keepdims=True), "cb")
    return lax.rsqrt(squares / model_width + epsilon)


def on_device(
    tokens,
    norm_gains,
    gate_weight,
    value_weight,
    gate_scale,
    value_scale,
    conv_gate,
    conv_value,
    down_weight,
    down_scale,
):
    model_width = lax.axis_size("cb") * tokens.shape[1]
    layer_count = gate_weight.shape[0]
    current = tokens
    for layer_idx in range(layer_count):
        state_wide = current.astype(jnp.float32)
        inverse = row_inverse(state_wide, model_width)
        scaled = (state_wide * norm_gains[layer_idx]).astype(jnp.bfloat16)
        gate_part = jnp.dot(
            scaled, gate_weight[layer_idx].astype(jnp.bfloat16), preferred_element_type=jnp.float32
        )
        value_part = jnp.dot(
            scaled, value_weight[layer_idx].astype(jnp.bfloat16), preferred_element_type=jnp.float32
        )
        gate_sum, value_sum = (
            lax.psum_scatter(gate_part, "cb", scatter_dimension=1, tiled=True),
            lax.psum_scatter(value_part, "cb", scatter_dimension=1, tiled=True),
        )
        share_cols = gate_sum.shape[1]
        first_col = lax.axis_index("cb") * share_cols
        gate_cols = lax.dynamic_slice_in_dim(gate_scale[layer_idx], first_col, share_cols, 0)
        value_cols = lax.dynamic_slice_in_dim(value_scale[layer_idx], first_col, share_cols, 0)
        gate_taps = lax.dynamic_slice_in_dim(conv_gate[layer_idx], first_col, share_cols, 1)
        value_taps = lax.dynamic_slice_in_dim(conv_value[layer_idx], first_col, share_cols, 1)
        gate_pre = inverse * gate_cols * gate_sum
        value_pre = inverse * value_cols * value_sum
        hidden = (
            jax.nn.gelu(causal_taps(gate_pre, gate_taps), approximate=True)
            * causal_taps(value_pre, value_taps)
        ).astype(jnp.bfloat16)
        hidden = lax.all_gather(hidden, "cb", axis=1, tiled=True)
        partial_value = jnp.dot(
            hidden, down_weight[layer_idx].astype(jnp.bfloat16), preferred_element_type=jnp.float32
        )
        down_total = lax.psum(partial_value, "ra")
        current = (residual_weight * state_wide + down_scale[layer_idx] * down_total).astype(
            jnp.bfloat16
        )
    state_wide = current.astype(jnp.float32)
    inverse = row_inverse(state_wide, model_width)
    return (state_wide * inverse * norm_gains[layer_count]).astype(jnp.bfloat16)


HALVES = 2
CORES = 2
LANES = 128
CHUNK = 256
RING = 12
STAGED = 5
BUBBLES = 12
PAIR_SUM, GATED, PAIR_GATHER, DOWN = 2, 5, 8, 10
Z_SUM, Z_GATHER, Z_SCALE = 8, 13, 14


def fused_kernel(
    ra_count,
    cb_count,
    tokens,
    gains,
    gate_hbm,
    value_hbm,
    gate_scale,
    value_scale,
    conv_gate,
    conv_value,
    down_hbm,
    down_scale,
    out,
    gate_stage,
    value_stage,
    down_stage,
    wide_weight,
    down_weight,
    current,
    scaled,
    inverse,
    padded,
    carry,
    pair_send,
    pair_recv,
    pair_own,
    x_send,
    x_recv,
    hidden,
    acc,
    z_send,
    z_recv,
    z_own,
    sq_send,
    sq_recv,
    gate_sem,
    value_sem,
    down_sem,
    pair_ss,
    pair_rs,
    x_ss,
    x_rs,
    hx_ss,
    hx_rs,
    hp_ss,
    hp_rs,
    z_ss,
    z_rs,
    c_ss,
    c_rs,
    sq_ss,
    sq_rs,
):
    f32, bf16 = jnp.float32, jnp.bfloat16
    layers = gate_hbm.shape[0]
    chunks = gate_hbm.shape[2] // CHUNK
    taps = conv_gate.shape[1]
    rows = tokens.shape[1]
    width = tokens.shape[2]
    model_width = width * cb_count
    x_count = cb_count // CORES
    block = rows // cb_count
    z_block = rows // ra_count
    period = HALVES * chunks + BUBBLES
    last_item = layers * period - BUBBLES
    streamed = layers * chunks

    me_cb = lax.axis_index("cb")
    me_ra = lax.axis_index("ra")
    me_x, me_core = lax.div(me_cb, CORES), lax.rem(me_cb, CORES)
    partner = me_x * CORES + (1 - me_core)

    def others(count, me):
        return [lax.rem(me + step, count) for step in range(1, count)]

    def remote(src, dst, send, recv, axis, index):
        return pltpu.make_async_remote_copy(
            src_ref=src,
            dst_ref=dst,
            send_sem=send,
            recv_sem=recv,
            device_id={axis: index},
            device_id_type=pl.DeviceIdType.MESH,
        )

    def cb_of(x_index):
        return x_index * CORES + me_core

    def wide_copies(n):
        layer, chunk, slot = lax.div(n, chunks), lax.rem(n, chunks), lax.rem(n, STAGED)
        cols = pl.ds(pl.multiple_of(chunk * CHUNK, CHUNK), CHUNK)
        return (
            pltpu.make_async_copy(gate_hbm.at[layer, :, cols], gate_stage.at[slot], gate_sem.at[slot]),
            pltpu.make_async_copy(value_hbm.at[layer, :, cols], value_stage.at[slot], value_sem.at[slot]),
        )

    def down_copy(n):
        layer, chunk, slot = lax.div(n, chunks), lax.rem(n, chunks), lax.rem(n, STAGED)
        cols = pl.ds(pl.multiple_of(chunk * CHUNK, CHUNK), CHUNK)
        return pltpu.make_async_copy(down_hbm.at[layer, cols, :], down_stage.at[slot], down_sem.at[slot])

    for n in range(min(STAGED, streamed)):
        for copy in wide_copies(n):
            copy.start()
        down_copy(n).start()

    barrier = pltpu.get_barrier_semaphore()
    for axis, count, me in (("cb", cb_count, me_cb), ("ra", ra_count, me_ra)):
        for peer in others(count, me):
            pl.semaphore_signal(
                barrier, inc=1, device_id={axis: peer}, device_id_type=pl.DeviceIdType.MESH
            )
    pl.semaphore_wait(barrier, cb_count + ra_count - 2)

    def pair_copy(slot):
        return remote(
            pair_send.at[slot], pair_recv.at[slot], pair_ss.at[slot], pair_rs.at[slot], "cb", partner
        )

    def x_copy(slot, peer, source):
        return remote(
            x_send.at[slot, peer],
            x_recv.at[slot, source],
            x_ss.at[slot, peer],
            x_rs.at[slot, source],
            "cb",
            cb_of(peer),
        )

    def hx_copy(slot, peer, source):
        place = hidden.at[slot, me_core * x_count + source]
        return remote(place, place, hx_ss.at[slot, peer], hx_rs.at[slot, source], "cb", cb_of(peer))

    def hp_copy(slot, core):
        place = hidden.at[slot, pl.ds(core * x_count, x_count)]
        return remote(place, place, hp_ss.at[slot], hp_rs.at[slot], "cb", partner)

    def z_copy(part, peer, source):
        return remote(
            z_send.at[part, peer],
            z_recv.at[part, source],
            z_ss.at[part, peer],
            z_rs.at[part, source],
            "ra",
            peer,
        )

    def c_copy(part, layer, half, peer, source):
        place = current.at[layer, half, source]
        return remote(place, place, c_ss.at[part, peer], c_rs.at[part, source], "ra", peer)

    def sq_copy(event, peer, source):
        return remote(
            sq_send.at[event], sq_recv.at[event, source], sq_ss.at[event, peer], sq_rs.at[event, source], "cb", peer
        )

    def scale_rows(layer, half):
        event = layer * HALVES + half
        wide = current[layer, half].reshape(rows, width).astype(f32)
        scaled[half] = (wide * gains[pl.ds(layer, 1), :]).astype(bf16)
        squares = jnp.sum(wide * wide, axis=1, keepdims=True)
        sq_send[event] = jnp.broadcast_to(squares, (rows, LANES)).T[:8]
        for peer in others(cb_count, me_cb):
            sq_copy(event, peer, me_cb).start()

    def finish_squares(layer, half):
        event = layer * HALVES + half
        total = sq_send[event]
        for peer in others(cb_count, me_cb):
            copy = sq_copy(event, peer, peer)
            copy.wait_send()
            copy.wait_recv()
            total = total + sq_recv[event, peer]
        row = lax.rsqrt(total / model_width + epsilon)
        inverse[half] = jnp.broadcast_to(row[:1], (LANES, rows)).T

    for half in range(HALVES):
        current[0, half] = tokens[half].reshape(ra_count, z_block, width)
        scale_rows(0, half)
    for half in range(HALVES):
        finish_squares(0, half)

    def place_of(item):
        layer, rest = lax.div(item, period), lax.rem(item, period)
        half, chunk = lax.div(rest, chunks), lax.rem(rest, chunks)
        ordinal = layer * (HALVES * chunks) + rest
        return layer, half, chunk, lax.rem(ordinal, RING)

    def project(layer, half, chunk, slot):
        n = layer * chunks + chunk

        @pl.when(half == 0)
        def _():
            stage = lax.rem(n, STAGED)
            for copy in wide_copies(n):
                copy.wait()
            wide_weight[chunk, :, :CHUNK] = gate_stage[stage].astype(bf16)
            wide_weight[chunk, :, CHUNK:] = value_stage[stage].astype(bf16)

            @pl.when(n + STAGED < streamed)
            def _():
                for copy in wide_copies(n + STAGED):
                    copy.start()

        product = jnp.dot(scaled[half], wide_weight[chunk], preferred_element_type=f32)
        inv = inverse[half]
        cols = pl.ds(pl.multiple_of(chunk * CHUNK, CHUNK), CHUNK)
        one = pl.ds(layer, 1)
        scales = jnp.concatenate([gate_scale[one, cols], value_scale[one, cols]], axis=1)
        weights = jnp.concatenate([conv_gate[layer, :, cols], conv_value[layer, :, cols]], axis=1)
        wide_inv = jnp.concatenate([inv] * (2 * CHUNK // LANES), axis=1)
        pre = product * wide_inv * scales
        before = carry[chunk]
        padded[:8] = jnp.where(half == 0, jnp.zeros_like(before), before)
        padded[8:] = pre
        carry[chunk] = pre[rows - 8 :]
        total = jnp.zeros_like(pre)
        for tap in range(taps):
            total = total + padded[pl.ds(8 - (taps - 1) + tap, rows), :] * weights[tap : tap + 1]
        part = rows // CORES
        for core in range(CORES):
            piece = total[core * part : (core + 1) * part]

            @pl.when(me_core == core)
            def _():
                pair_own[slot] = piece.reshape(x_count, block, 2 * CHUNK)

            @pl.when(me_core != core)
            def _():
                pair_send[slot] = piece.astype(bf16).reshape(x_count, block, 2 * CHUNK)

        pair_copy(slot).start()

    def pair_sum(layer, half, chunk, slot):
        pair_copy(slot).wait()
        both = pair_own[slot] + pair_recv[slot].astype(f32)
        pair_own[slot] = both
        x_send[slot] = both.astype(bf16)
        for peer in others(x_count, me_x):
            x_copy(slot, peer, me_x).start()

    def gated(layer, half, chunk, slot):
        total = pair_own[slot, me_x]
        for peer in others(x_count, me_x):
            copy = x_copy(slot, peer, peer)
            copy.wait_send()
            copy.wait_recv()
            total = total + x_recv[slot, peer].astype(f32)
        unit = jax.nn.gelu(total[:, :CHUNK], approximate=True) * total[:, CHUNK:]
        hidden[slot, me_core * x_count + me_x] = unit.astype(bf16)
        for peer in others(x_count, me_x):
            hx_copy(slot, peer, me_x).start()

    def pair_gather(layer, half, chunk, slot):
        for peer in others(x_count, me_x):
            hx_copy(slot, peer, me_x).wait_send()
            hx_copy(slot, peer, peer).wait_recv()
        hp_copy(slot, me_core).start()

    def project_down(layer, half, chunk, slot):
        n = layer * chunks + chunk

        @pl.when(half == 0)
        def _():
            stage = lax.rem(n, STAGED)
            down_copy(n).wait()
            down_weight[chunk] = down_stage[stage].astype(bf16)

            @pl.when(n + STAGED < streamed)
            def _():
                down_copy(n + STAGED).start()

        hp_copy(slot, me_core).wait_send()
        hp_copy(slot, 1 - me_core).wait_recv()
        product = jnp.dot(
            hidden[slot].reshape(rows, CHUNK), down_weight[chunk], preferred_element_type=f32
        ).reshape(ra_count, z_block, width)

        @pl.when(chunk == 0)
        def _():
            acc[...] = product

        @pl.when(chunk > 0)
        def _():
            acc[...] += product

        @pl.when(chunk == chunks - 1)
        def _():
            part = layer * HALVES + half
            z_send[part] = acc[...].astype(bf16)
            z_own[part] = acc[me_ra]
            for peer in others(ra_count, me_ra):
                z_copy(part, peer, me_ra).start()

    def z_sum(layer, half, chunk, slot):
        part = layer * HALVES + half
        total = z_own[part]
        for peer in others(ra_count, me_ra):
            copy = z_copy(part, peer, peer)
            copy.wait_send()
            copy.wait_recv()
            total = total + z_recv[part, peer].astype(f32)
        kept = residual_weight * current[layer, half, me_ra].astype(f32)
        current[layer + 1, half, me_ra] = (kept + down_scale[pl.ds(layer, 1), :] * total).astype(bf16)
        for peer in others(ra_count, me_ra):
            c_copy(part, layer + 1, half, peer, me_ra).start()

    def z_gather(layer, half, chunk, slot):
        part = layer * HALVES + half
        for peer in others(ra_count, me_ra):
            c_copy(part, layer + 1, half, peer, me_ra).wait_send()
            c_copy(part, layer + 1, half, peer, peer).wait_recv()
        scale_rows(layer + 1, half)

    def z_scale(layer, half, chunk, slot):
        finish_squares(layer + 1, half)

        @pl.when(layer == layers - 1)
        def _():
            wide = current[layers, half].reshape(rows, width).astype(f32)
            inv = jnp.concatenate([inverse[half]] * (width // LANES), axis=1)
            out[half] = (wide * inv * gains[pl.ds(layers, 1), :]).astype(bf16)

    stages = (
        (DOWN + Z_SCALE, True, z_scale),
        (DOWN + Z_GATHER, True, z_gather),
        (DOWN + Z_SUM, True, z_sum),
        (PAIR_GATHER, False, pair_gather),
        (GATED, False, gated),
        (PAIR_SUM, False, pair_sum),
        (0, False, project),
        (DOWN, False, project_down),
    )
    assert DOWN + Z_SCALE <= chunks + BUBBLES + 1

    def step(index, _):
        for delay, at_end, stage in stages:
            item = index - delay
            rest = lax.rem(item + period, period)
            valid = (item >= 0) & (item < last_item) & (rest < HALVES * chunks)
            if at_end:
                valid = valid & (lax.rem(rest, chunks) == chunks - 1)

            @pl.when(valid)
            def _(stage=stage, item=item):
                stage(*place_of(item))

        return 0

    lax.fori_loop(0, last_item + DOWN + Z_SCALE, step, 0)


def fits(ra_count, cb_count, tokens, gate_weight, conv_gate):
    rows = tokens.shape[0] // HALVES
    return (
        cb_count % CORES == 0
        and cb_count > CORES
        and ra_count > 1
        and tokens.shape[0] % HALVES == 0
        and rows % LANES == 0
        and (rows // LANES) == 1
        and rows % (16 * cb_count) == 0
        and rows % (16 * ra_count) == 0
        and tokens.shape[1] % LANES == 0
        and gate_weight.shape[2] % CHUNK == 0
        and gate_weight.shape[2] // CHUNK + BUBBLES + 1 >= DOWN + Z_SCALE
        and conv_gate.shape[1] <= 9
    )


def on_device_any(ra_count, cb_count, *args):
    (
        tokens,
        norm_gains,
        gate_weight,
        value_weight,
        gate_scale,
        value_scale,
        conv_gate,
        conv_value,
        down_weight,
        down_scale,
    ) = args
    if not fits(ra_count, cb_count, tokens, gate_weight, conv_gate):
        return on_device(*args)
    f32, bf16 = jnp.float32, jnp.bfloat16
    layers, width, units = gate_weight.shape
    rows = tokens.shape[0] // HALVES
    chunks = units // CHUNK
    x_count = cb_count // CORES
    block, z_block = rows // cb_count, rows // ra_count
    parts, events = layers * HALVES, (layers + 1) * HALVES
    vmem, dma = pltpu.VMEM, pltpu.SemaphoreType.DMA
    in_vmem, in_hbm = pl.BlockSpec(memory_space=pltpu.VMEM), pl.BlockSpec(memory_space=pl.ANY)
    result = pl.pallas_call(
        functools.partial(fused_kernel, ra_count, cb_count),
        out_shape=jax.ShapeDtypeStruct((HALVES, rows, width), bf16),
        in_specs=[in_vmem, in_vmem, in_hbm, in_hbm] + [in_vmem] * 4 + [in_hbm, in_vmem],
        out_specs=in_vmem,
        scratch_shapes=[
            vmem((STAGED, width, CHUNK), f32),
            vmem((STAGED, width, CHUNK), f32),
            vmem((STAGED, CHUNK, width), f32),
            vmem((chunks, width, 2 * CHUNK), bf16),
            vmem((chunks, CHUNK, width), bf16),
            vmem((layers + 1, HALVES, ra_count, z_block, width), bf16),
            vmem((HALVES, rows, width), bf16),
            vmem((HALVES, rows, LANES), f32),
            vmem((rows + 8, 2 * CHUNK), f32),
            vmem((chunks, 8, 2 * CHUNK), f32),
            vmem((RING, x_count, block, 2 * CHUNK), bf16),
            vmem((RING, x_count, block, 2 * CHUNK), bf16),
            vmem((RING, x_count, block, 2 * CHUNK), f32),
            vmem((RING, x_count, block, 2 * CHUNK), bf16),
            vmem((RING, x_count, block, 2 * CHUNK), bf16),
            vmem((RING, cb_count, block, CHUNK), bf16),
            vmem((ra_count, z_block, width), f32),
            vmem((parts, ra_count, z_block, width), bf16),
            vmem((parts, ra_count, z_block, width), bf16),
            vmem((parts, z_block, width), f32),
            vmem((events, 8, rows), f32),
            vmem((events, cb_count, 8, rows), f32),
            dma((STAGED,)),
            dma((STAGED,)),
            dma((STAGED,)),
            dma((RING,)),
            dma((RING,)),
            dma((RING, x_count)),
            dma((RING, x_count)),
            dma((RING, x_count)),
            dma((RING, x_count)),
            dma((RING,)),
            dma((RING,)),
            dma((parts, ra_count)),
            dma((parts, ra_count)),
            dma((parts, ra_count)),
            dma((parts, ra_count)),
            dma((events, cb_count)),
            dma((events, cb_count)),
        ],
        compiler_params=pltpu.CompilerParams(
            collective_id=0, has_side_effects=True, vmem_limit_bytes=62 * 1024 * 1024
        ),
        name="fused_sublayers",
    )(
        tokens.reshape(HALVES, rows, width),
        norm_gains,
        gate_weight,
        value_weight,
        gate_scale,
        value_scale,
        conv_gate,
        conv_value,
        down_weight,
        down_scale,
    )
    return result.reshape(HALVES * rows, width)


def solution(mesh):
    in_specs = (
        P("grp", "cb"),
        P(None, "cb"),
        P(None, "cb", "ra"),
        P(None, "cb", "ra"),
        P(None, "ra"),
        P(None, "ra"),
        P(None, None, "ra"),
        P(None, None, "ra"),
        P(None, "ra", "cb"),
        P(None, "cb"),
    )
    out_specs = P("grp", "cb")
    return jax.shard_map(
        functools.partial(on_device_any, mesh.shape["ra"], mesh.shape["cb"]), mesh=mesh, in_specs=in_specs, out_specs=out_specs, check_vma=False
    )
```

profile of v0, /device:TPU:0, one launch (start us, length us, event | category | flops | bytes accessed | tf_op | source)
XLA Modules:
  0.0 112.3 jit_solution(13095200637353050316)
XLA Ops:
  0.0 1.5 %copy.11.conv_gate = f32[2,3,2816]{2,1,0:T(4,128)} copy(f32[2,3,2816]{2,0,1:T(2,128)} %param.16) | data formatting | bytes 135168 | tf_op args[6]
  1.5 1.5 %copy.12.conv_value = f32[2,3,2816]{2,1,0:T(4,128)} copy(f32[2,3,2816]{2,0,1:T(2,128)} %param.17) | data formatting | bytes 135168 | tf_op args[7]
  3.1 107.3 %fused_sublayers.1 = bf16[2,128,1024]{2,1,0:T(8,128)(2,1)} custom-call(bf16[2,128,1024]{2,1,0:T(8,128)(2,1)} %bitcast.3, f32[3,1024]{1,0:T(4,128)} %gains.1, f32[2,1024,2816]{2,1,0:T(8,128)} %gate_hbm.1, f32[2,1024,2816]{2,1,0:T(8,128)} %value_hbm.1, f32[2,2816]{1,0:T(2,128)} %gate_scale.1, f32[2,2816]{1,0:T(2,128)} %value_scale.1, ...), custom_call_target="tpu_custom_call" | custom-call | tf_op jit(solution)/shard_map/fused_sublayers/pallas_call | solution.py:489
  110.4 1.9 %copy.14 = bf16[256,1024]{1,0:T(8,128)(2,1)} copy(bf16[256,1024]{1,0:T(8,128)(2,1)} %bitcast.2) | data formatting | bytes 1048576
where the time goes:
time: 113 us; the launch traced here: 112 us
  Pallas kernels  107 us (95%)
  local copies, waits for them, and re-layouts  4.95 us (4%)
    pallas_call x1, Pallas kernels, on_device_any(): pl.pallas_call(functools.partial(fused_kernel, ra_count, cb_count), out_s...  107 us
    unnamed x3, local copies, waits for them, and re-layouts  4.95 us

commit v1 on v0

v1 whole, which is shorter than its diff:
```python
import functools

import jax
import jax.numpy as jnp
from jax import lax
from jax.experimental import pallas as pl
from jax.experimental.pallas import tpu as pltpu
from jax.sharding import PartitionSpec as P

epsilon = 1e-06
residual_weight = 0.5


def causal_taps(projected, tap_weights):
    tap_count = tap_weights.shape[0]
    row_count = projected.shape[0]
    padded = jnp.pad(projected, ((tap_count - 1, 0), (0, 0)))
    result = jnp.zeros_like(projected)
    for tap_idx in range(tap_count):
        result = result + padded[tap_idx : tap_idx + row_count] * tap_weights[tap_idx]
    return result


def row_inverse(state_wide, model_width):
    squares = lax.psum(jnp.sum(state_wide * state_wide, axis=1, keepdims=True), "cb")
    return lax.rsqrt(squares / model_width + epsilon)


def on_device(
    tokens,
    norm_gains,
    gate_weight,
    value_weight,
    gate_scale,
    value_scale,
    conv_gate,
    conv_value,
    down_weight,
    down_scale,
):
    model_width = lax.axis_size("cb") * tokens.shape[1]
    layer_count = gate_weight.shape[0]
    current = tokens
    for layer_idx in range(layer_count):
        state_wide = current.astype(jnp.float32)
        inverse = row_inverse(state_wide, model_width)
        scaled = (state_wide * norm_gains[layer_idx]).astype(jnp.bfloat16)
        gate_part = jnp.dot(
            scaled, gate_weight[layer_idx].astype(jnp.bfloat16), preferred_element_type=jnp.float32
        )
        value_part = jnp.dot(
            scaled, value_weight[layer_idx].astype(jnp.bfloat16), preferred_element_type=jnp.float32
        )
        gate_sum, value_sum = (
            lax.psum_scatter(gate_part, "cb", scatter_dimension=1, tiled=True),
            lax.psum_scatter(value_part, "cb", scatter_dimension=1, tiled=True),
        )
        share_cols = gate_sum.shape[1]
        first_col = lax.axis_index("cb") * share_cols
        gate_cols = lax.dynamic_slice_in_dim(gate_scale[layer_idx], first_col, share_cols, 0)
        value_cols = lax.dynamic_slice_in_dim(value_scale[layer_idx], first_col, share_cols, 0)
        gate_taps = lax.dynamic_slice_in_dim(conv_gate[layer_idx], first_col, share_cols, 1)
        value_taps = lax.dynamic_slice_in_dim(conv_value[layer_idx], first_col, share_cols, 1)
        gate_pre = inverse * gate_cols * gate_sum
        value_pre = inverse * value_cols * value_sum
        hidden = (
            jax.nn.gelu(causal_taps(gate_pre, gate_taps), approximate=True)
            * causal_taps(value_pre, value_taps)
        ).astype(jnp.bfloat16)
        hidden = lax.all_gather(hidden, "cb", axis=1, tiled=True)
        partial_value = jnp.dot(
            hidden, down_weight[layer_idx].astype(jnp.bfloat16), preferred_element_type=jnp.float32
        )
        down_total = lax.psum(partial_value, "ra")
        current = (residual_weight * state_wide + down_scale[layer_idx] * down_total).astype(
            jnp.bfloat16
        )
    state_wide = current.astype(jnp.float32)
    inverse = row_inverse(state_wide, model_width)
    return (state_wide * inverse * norm_gains[layer_count]).astype(jnp.bfloat16)


CORES = 2
LANES = 128
GROUP = 64
RING = 13
WIDE_SLOTS = 16
DOWN_SLOTS = 16
FIRST_LOADS = 6
DOWN_LAG = 3
BUBBLES = 3
PAIR_SUM, GATED, PAIR_GATHER, DOWN = 2, 5, 8, 10
Z_SUM, Z_GATHER, Z_SCALE = 6, 12, 13


def fused_kernel(
    ra_count,
    cb_count,
    tokens,
    gains,
    gate_hbm,
    value_hbm,
    gate_scale,
    value_scale,
    conv_gate,
    conv_value,
    down_hbm,
    down_scale,
    out,
    wide_weight,
    down_weight,
    current,
    scaled,
    inverse,
    padded,
    carry,
    pair_send,
    pair_recv,
    pair_own,
    x_send,
    x_recv,
    hidden,
    acc,
    z_send,
    z_recv,
    z_own,
    sq_send,
    sq_recv,
    wide_sem,
    down_sem,
    pair_ss,
    pair_rs,
    x_ss,
    x_rs,
    hx_ss,
    hx_rs,
    hp_ss,
    hp_rs,
    z_ss,
    z_rs,
    c_ss,
    c_rs,
    sq_ss,
    sq_rs,
):
    f32, bf16 = jnp.float32, jnp.bfloat16
    layers = gate_hbm.shape[0]
    groups = tokens.shape[0]
    rows = tokens.shape[1]
    width = tokens.shape[2]
    x_count = cb_count // CORES
    chunk_cols = x_count * LANES
    chunks = gate_hbm.shape[2] // chunk_cols
    pairs = pl.cdiv(chunks, CORES)
    taps = conv_gate.shape[0]
    model_width = width * cb_count
    z_block = rows // ra_count
    per_layer = groups * pairs
    period = per_layer + BUBBLES
    last_item = layers * period - BUBBLES
    all_groups = groups + (BUBBLES > 0)
    streamed = layers * chunks

    me_cb = lax.axis_index("cb")
    me_ra = lax.axis_index("ra")
    me_x, me_core = lax.div(me_cb, CORES), lax.rem(me_cb, CORES)
    partner = me_x * CORES + (1 - me_core)

    def others(count, me):
        return [lax.rem(me + step, count) for step in range(1, count)]

    def remote(src, dst, send, recv, axis, index):
        return pltpu.make_async_remote_copy(
            src_ref=src,
            dst_ref=dst,
            send_sem=send,
            recv_sem=recv,
            device_id={axis: index},
            device_id_type=pl.DeviceIdType.MESH,
        )

    cb_peers, ra_peers, x_peers = others(cb_count, me_cb), others(ra_count, me_ra), others(x_count, me_x)

    def cb_of(x_index):
        return x_index * CORES + me_core

    def place_of(n):
        layer = sum((jnp.asarray(n >= later * chunks).astype(jnp.int32) for later in range(1, layers)), 0)
        return layer, n - layer * chunks

    def wide_copies(n):
        (layer, chunk), slot = place_of(n), lax.rem(n, WIDE_SLOTS)
        cols = pl.ds(pl.multiple_of(chunk * chunk_cols, chunk_cols), chunk_cols)
        return (
            pltpu.make_async_copy(
                gate_hbm.at[layer, :, cols],
                wide_weight.at[slot, :, pl.ds(0, chunk_cols)],
                wide_sem.at[slot, 0],
            ),
            pltpu.make_async_copy(
                value_hbm.at[layer, :, cols],
                wide_weight.at[slot, :, pl.ds(chunk_cols, chunk_cols)],
                wide_sem.at[slot, 1],
            ),
        )

    def down_copies(n):
        (layer, chunk), slot = place_of(n), lax.rem(n, DOWN_SLOTS)
        cols = pl.ds(pl.multiple_of(chunk * chunk_cols, chunk_cols), chunk_cols)
        return (
            pltpu.make_async_copy(down_hbm.at[layer, cols, :], down_weight.at[slot], down_sem.at[slot]),
        )

    def start_copies(copies, n, limit):
        @pl.when(n < limit)
        def _():
            for copy in copies(n):
                copy.start()

    for n in range(min(FIRST_LOADS, streamed)):
        for copy in wide_copies(n):
            copy.start()

    barrier = pltpu.get_barrier_semaphore()
    for axis, count, me in (("cb", cb_count, me_cb), ("ra", ra_count, me_ra)):
        for peer in others(count, me):
            pl.semaphore_signal(
                barrier, inc=1, device_id={axis: peer}, device_id_type=pl.DeviceIdType.MESH
            )
    pl.semaphore_wait(barrier, cb_count + ra_count - 2)

    def pair_copy(slot):
        return remote(
            pair_send.at[slot], pair_recv.at[slot], pair_ss.at[slot], pair_rs.at[slot], "cb", partner
        )

    def x_copy(slot, peer, source):
        return remote(
            x_send.at[slot, peer],
            x_recv.at[slot, source],
            x_ss.at[slot, peer],
            x_rs.at[slot, source],
            "cb",
            cb_of(peer),
        )

    def hx_copy(slot, peer, source):
        place = hidden.at[slot, me_core * x_count + source]
        return remote(place, place, hx_ss.at[slot, peer], hx_rs.at[slot, source], "cb", cb_of(peer))

    def hp_copy(slot, core):
        place = hidden.at[slot, pl.ds(core * x_count, x_count)]
        return remote(place, place, hp_ss.at[slot], hp_rs.at[slot], "cb", partner)

    def z_copy(part, peer, source):
        return remote(
            z_send.at[part, peer],
            z_recv.at[part, source],
            z_ss.at[part, peer],
            z_rs.at[part, source],
            "ra",
            peer,
        )

    def c_copy(part, layer, group, peer, source):
        place = current.at[layer, group, source]
        return remote(place, place, c_ss.at[part, peer], c_rs.at[part, source], "ra", peer)

    def sq_copy(event, peer, source):
        return remote(
            sq_send.at[event], sq_recv.at[event, source], sq_ss.at[event, peer], sq_rs.at[event, source], "cb", peer
        )

    def scale_rows(layer, group):
        event = layer * groups + group
        wide = current[layer, group].reshape(rows, width).astype(f32)
        scaled[group] = (wide * gains[pl.ds(layer, 1), :]).astype(bf16).astype(f32)
        squares = jnp.broadcast_to(jnp.sum(wide * wide, axis=1, keepdims=True), (rows, LANES))
        sq_send[event] = jnp.concatenate([squares] * (LANES // rows), axis=0).T[:8]
        for peer in cb_peers:
            sq_copy(event, peer, me_cb).start()

    def finish_squares(layer, group):
        event = layer * groups + group
        total = sq_send[event]
        for peer in cb_peers:
            copy = sq_copy(event, peer, peer)
            copy.wait_send()
            copy.wait_recv()
            total = total + sq_recv[event, peer]
        row = lax.rsqrt(total / model_width + epsilon)
        inverse[group] = jnp.broadcast_to(row[:1], (LANES, LANES)).T[:rows]

    for group in range(groups):
        current[0, group] = tokens[group].reshape(ra_count, z_block, width)
        scale_rows(0, group)

    def when_full(pair, both, first_only):
        if chunks % CORES == 0:
            both()
        else:
            pl.when(pair < pairs - 1)(both)
            pl.when(pair == pairs - 1)(first_only)

    def when_owner(pair, fn):
        if chunks % CORES == 0:
            fn()
        else:
            pl.when((pair < pairs - 1) | (me_core == 0))(fn)

    def when_partner(pair, fn):
        if chunks % CORES == 0:
            fn()
        else:
            pl.when((pair < pairs - 1) | (me_core == 1))(fn)

    def project(layer, group, pair, slot):
        ordinal = group * pairs + pair
        first = layer * chunks + pair * CORES
        end = (layer + 1) * chunks

        @pl.when(layer == 0)
        def _():
            for n in range(CORES):
                start_copies(wide_copies, FIRST_LOADS + ordinal * CORES + n, min(WIDE_SLOTS, streamed))

            @pl.when(ordinal >= DOWN_LAG)
            def _():
                for n in range(CORES):
                    start_copies(down_copies, (ordinal - DOWN_LAG) * CORES + n, min(DOWN_SLOTS, streamed))

        @pl.when(group == 0)
        def _():
            for n in range(CORES):

                @pl.when(first + n < end)
                def _(n=n):
                    for copy in wide_copies(first + n):
                        copy.wait()

        def product_of(chunk_at):
            return jnp.dot(
                scaled[group], wide_weight[lax.rem(chunk_at, WIDE_SLOTS)], preferred_element_type=f32
            )

        def keep(chunk_at):
            product = product_of(chunk_at)
            for x in range(x_count):
                for kind in range(2):
                    at = kind * chunk_cols + x * LANES
                    pair_own[slot, x, :, kind * LANES : (kind + 1) * LANES] = product[:, at : at + LANES]

        def give(chunk_at):
            product = product_of(chunk_at)
            for x in range(x_count):
                for kind in range(2):
                    at = kind * chunk_cols + x * LANES
                    pair_send[slot, x, :, kind * LANES : (kind + 1) * LANES] = product[
                        :, at : at + LANES
                    ].astype(bf16)

        def both():
            give(first + 1 - me_core)
            pair_copy(slot).start()
            keep(first + me_core)

        def first_only():
            @pl.when(me_core == 0)
            def _():
                keep(first)

            @pl.when(me_core == 1)
            def _():
                give(first)
                pair_copy(slot).start()

        when_full(pair, both, first_only)

        @pl.when(group == groups - 1)
        def _():
            for n in range(CORES):

                @pl.when(first + n < end)
                def _(n=n):
                    start_copies(wide_copies, first + n + WIDE_SLOTS, streamed)

    def pair_sum(layer, group, pair, slot):
        when_partner(pair, lambda: pair_copy(slot).wait_send())

        def send():
            pair_copy(slot).wait_recv()
            for peer in x_peers:
                x_send[slot, peer] = (pair_own[slot, peer] + pair_recv[slot, peer].astype(f32)).astype(bf16)
                x_copy(slot, peer, me_x).start()

        when_owner(pair, send)

    def gated(layer, group, pair, slot):
        @pl.when(pair == 0)
        def _():
            finish_squares(layer, group)

        def unit():
            total = pair_own[slot, me_x] + pair_recv[slot, me_x].astype(f32)
            for peer in x_peers:
                copy = x_copy(slot, peer, peer)
                copy.wait_send()
                copy.wait_recv()
                total = total + x_recv[slot, peer].astype(f32)
            at = (pair * CORES + me_core) * chunk_cols
            cols = pl.ds(pl.multiple_of(at, chunk_cols), chunk_cols)
            one = pl.ds(layer, 1)

            def mine(values):
                kept = values[:, :LANES]
                for x in range(1, x_count):
                    kept = jnp.where(me_x == x, values[:, x * LANES : (x + 1) * LANES], kept)
                return kept

            scales = jnp.concatenate([mine(gate_scale[one, cols]), mine(value_scale[one, cols])], axis=1)
            weights = jnp.concatenate(
                [mine(conv_gate[:, layer, cols]), mine(conv_value[:, layer, cols])], axis=1
            )
            inv = inverse[group]
            pre = total * jnp.concatenate([inv, inv], axis=1) * scales
            before = carry[pair]
            padded[:8] = jnp.where(group == 0, jnp.zeros_like(before), before)
            padded[8:] = pre
            carry[pair] = pre[rows - 8 :]
            mixed = pre * weights[taps - 1 : taps]
            for tap in range(taps - 1):
                mixed = mixed + padded[pl.ds(8 - (taps - 1) + tap, rows), :] * weights[tap : tap + 1]
            hidden[slot, me_core * x_count + me_x] = (
                jax.nn.gelu(mixed[:, :LANES], approximate=True) * mixed[:, LANES:]
            ).astype(bf16)
            for peer in x_peers:
                hx_copy(slot, peer, me_x).start()

        when_owner(pair, unit)

    def pair_gather(layer, group, pair, slot):
        def forward():
            for peer in x_peers:
                hx_copy(slot, peer, me_x).wait_send()
                hx_copy(slot, peer, peer).wait_recv()
            hp_copy(slot, me_core).start()

        when_owner(pair, forward)

    def project_down(layer, group, pair, slot):
        first = layer * chunks + pair * CORES
        end = (layer + 1) * chunks

        @pl.when(group == 0)
        def _():
            for n in range(CORES):

                @pl.when(first + n < end)
                def _(n=n):
                    for copy in down_copies(first + n):
                        copy.wait()

        when_owner(pair, lambda: hp_copy(slot, me_core).wait_send())
        when_partner(pair, lambda: hp_copy(slot, 1 - me_core).wait_recv())

        def add(count):
            left = jnp.concatenate([hidden[slot, n] for n in range(count * x_count)], axis=1).astype(f32)
            right = jnp.concatenate(
                [down_weight[lax.rem(first + n, DOWN_SLOTS)] for n in range(count)], axis=0
            )
            product = jnp.dot(left, right, preferred_element_type=f32)
            before = acc[...]
            acc[...] = jnp.where(pair == 0, jnp.zeros_like(before), before) + product

        when_full(pair, lambda: add(CORES), lambda: add(1))

        @pl.when(group == groups - 1)
        def _():
            for n in range(CORES):

                @pl.when(first + n < end)
                def _(n=n):
                    start_copies(down_copies, first + n + DOWN_SLOTS, streamed)

        @pl.when(pair == pairs - 1)
        def _():
            part = layer * groups + group
            total = acc[...].reshape(ra_count, z_block, width)
            z_send[part] = total.astype(bf16)
            z_own[part] = acc[pl.ds(pl.multiple_of(me_ra * z_block, z_block), z_block), :]
            for peer in ra_peers:
                z_copy(part, peer, me_ra).start()

    def z_sum(layer, group, pair, slot):
        part = layer * groups + group
        total = z_own[part]
        for peer in ra_peers:
            copy = z_copy(part, peer, peer)
            copy.wait_send()
            copy.wait_recv()
            total = total + z_recv[part, peer].astype(f32)
        kept = residual_weight * current[layer, group, me_ra].astype(f32)
        current[layer + 1, group, me_ra] = (kept + down_scale[pl.ds(layer, 1), :] * total).astype(bf16)
        for peer in ra_peers:
            c_copy(part, layer + 1, group, peer, me_ra).start()

    def z_gather(layer, group, pair, slot):
        part = layer * groups + group
        for peer in ra_peers:
            c_copy(part, layer + 1, group, peer, me_ra).wait_send()
            c_copy(part, layer + 1, group, peer, peer).wait_recv()
        scale_rows(layer + 1, group)

    def z_scale(layer, group, pair, slot):
        @pl.when(layer == layers - 1)
        def _():
            finish_squares(layers, group)
            wide = current[layers, group].reshape(rows, width).astype(f32)
            inv = jnp.concatenate([inverse[group]] * (width // LANES), axis=1)
            out[group] = (wide * inv * gains[pl.ds(layers, 1), :]).astype(bf16)

    stages = (
        (DOWN + Z_SCALE, True, z_scale),
        (DOWN + Z_GATHER, True, z_gather),
        (DOWN + Z_SUM, True, z_sum),
        (PAIR_GATHER, False, pair_gather),
        (GATED, False, gated),
        (PAIR_SUM, False, pair_sum),
        (0, False, project),
        (DOWN, False, project_down),
    )

    delays = sorted({delay for delay, _, _ in stages})

    def started(delay):
        layer, rest = divmod(-delay, period)
        group, pair = (groups, rest - per_layer) if rest >= per_layer else divmod(rest, pairs)
        return tuple(jnp.int32(value) for value in (layer, group, pair, 0))

    def advanced(place):
        layer, group, pair, slot = place
        used = (layer >= 0) & (group < groups)
        slot = jnp.where(used, jnp.where(slot == RING - 1, 0, slot + 1), slot)
        wrap = pair + 1 == jnp.where(group == groups, BUBBLES, pairs)
        pair = jnp.where(wrap, 0, pair + 1)
        group = jnp.where(wrap, group + 1, group)
        next_layer = group == all_groups
        return jnp.where(next_layer, layer + 1, layer), jnp.where(next_layer, 0, group), pair, slot

    def step(index, places):
        for delay, at_end, stage in stages:
            place = places[delays.index(delay)]
            layer, group, pair, slot = place
            valid = (layer >= 0) & (layer < layers) & (group < groups)
            if at_end:
                valid = valid & (pair == pairs - 1)

            @pl.when(valid)
            def _(stage=stage, place=place):
                stage(*place)

        return tuple(advanced(place) for place in places)

    lax.fori_loop(0, last_item + DOWN + Z_SCALE, step, tuple(started(delay) for delay in delays))


def fits(ra_count, cb_count, tokens, gate_weight, conv_gate):
    rows, width = tokens.shape
    layers, _, units = gate_weight.shape
    if cb_count % CORES or cb_count <= CORES or ra_count < 2 or rows % GROUP or GROUP % (16 * ra_count):
        return False
    chunk_cols = cb_count // CORES * LANES
    if width % LANES or units % chunk_cols or units // chunk_cols < CORES or conv_gate.shape[1] > 9:
        return False
    chunks = units // chunk_cols
    pairs, groups = pl.cdiv(chunks, CORES), rows // GROUP
    weights = 4 * width * chunk_cols * (2 * WIDE_SLOTS + DOWN_SLOTS)
    return (
        chunks <= min(WIDE_SLOTS, DOWN_SLOTS)
        and (groups - 1) * pairs + 1 + BUBBLES >= DOWN + Z_GATHER
        and weights + 4 * rows * width * 12 <= 60 * 1024 * 1024
    )


def on_device_any(ra_count, cb_count, *args):
    (
        tokens,
        norm_gains,
        gate_weight,
        value_weight,
        gate_scale,
        value_scale,
        conv_gate,
        conv_value,
        down_weight,
        down_scale,
    ) = args
    if not fits(ra_count, cb_count, tokens, gate_weight, conv_gate):
        return on_device(*args)
    f32, bf16 = jnp.float32, jnp.bfloat16
    layers, width, units = gate_weight.shape
    groups, rows = tokens.shape[0] // GROUP, GROUP
    x_count = cb_count // CORES
    chunk_cols = x_count * LANES
    pairs = pl.cdiv(units // chunk_cols, CORES)
    z_block = rows // ra_count
    parts, events = layers * groups, (layers + 1) * groups
    vmem, dma = pltpu.VMEM, pltpu.SemaphoreType.DMA
    in_vmem, in_hbm = pl.BlockSpec(memory_space=pltpu.VMEM), pl.BlockSpec(memory_space=pl.ANY)
    result = pl.pallas_call(
        functools.partial(fused_kernel, ra_count, cb_count),
        out_shape=jax.ShapeDtypeStruct((groups, rows, width), bf16),
        in_specs=[in_vmem, in_vmem, in_hbm, in_hbm] + [in_vmem] * 4 + [in_hbm, in_vmem],
        out_specs=in_vmem,
        scratch_shapes=[
            vmem((WIDE_SLOTS, width, 2 * chunk_cols), f32),
            vmem((DOWN_SLOTS, chunk_cols, width), f32),
            vmem((layers + 1, groups, ra_count, z_block, width), bf16),
            vmem((groups, rows, width), f32),
            vmem((groups, rows, LANES), f32),
            vmem((rows + 8, 2 * LANES), f32),
            vmem((pairs, 8, 2 * LANES), f32),
            vmem((RING, x_count, rows, 2 * LANES), bf16),
            vmem((RING, x_count, rows, 2 * LANES), bf16),
            vmem((RING, x_count, rows, 2 * LANES), f32),
            vmem((RING, x_count, rows, 2 * LANES), bf16),
            vmem((RING, x_count, rows, 2 * LANES), bf16),
            vmem((RING, cb_count, rows, LANES), bf16),
            vmem((rows, width), f32),
            vmem((parts, ra_count, z_block, width), bf16),
            vmem((parts, ra_count, z_block, width), bf16),
            vmem((parts, z_block, width), f32),
            vmem((events, 8, LANES), f32),
            vmem((events, cb_count, 8, LANES), f32),
            dma((WIDE_SLOTS, 2)),
            dma((DOWN_SLOTS,)),
            dma((RING,)),
            dma((RING,)),
            dma((RING, x_count)),
            dma((RING, x_count)),
            dma((RING, x_count)),
            dma((RING, x_count)),
            dma((RING,)),
            dma((RING,)),
            dma((parts, ra_count)),
            dma((parts, ra_count)),
            dma((parts, ra_count)),
            dma((parts, ra_count)),
            dma((events, cb_count)),
            dma((events, cb_count)),
        ],
        compiler_params=pltpu.CompilerParams(
            collective_id=0, has_side_effects=True, vmem_limit_bytes=67043328
        ),
        name="fused_sublayers",
    )(
        tokens.reshape(groups, rows, width),
        norm_gains,
        gate_weight,
        value_weight,
        gate_scale,
        value_scale,
        conv_gate.transpose(1, 0, 2),
        conv_value.transpose(1, 0, 2),
        down_weight,
        down_scale,
    )
    return result.reshape(groups * rows, width)


def solution(mesh):
    in_specs = (
        P("grp", "cb"),
        P(None, "cb"),
        P(None, "cb", "ra"),
        P(None, "cb", "ra"),
        P(None, "ra"),
        P(None, "ra"),
        P(None, None, "ra"),
        P(None, None, "ra"),
        P(None, "ra", "cb"),
        P(None, "cb"),
    )
    out_specs = P("grp", "cb")
    return jax.shard_map(
        functools.partial(on_device_any, mesh.shape["ra"], mesh.shape["cb"]), mesh=mesh, in_specs=in_specs, out_specs=out_specs, check_vma=False
    )
```

time: 113 us -> 99.1 us (0.88)
  Pallas kernels: 107 us -> 97 us
  local copies, waits for them, and re-layouts: 4.95 us -> 1.87 us
    pallas_call x1, Pallas kernels: 107 us -> 97 us  [on_device_any(): pl.pallas_call(functools.partial(fused_kernel, ra_count, cb_count), out_s...]
    unnamed x3 -> x1, local copies, waits for them, and re-layouts: 4.95 us -> 1.87 us
where the time goes in v1:
time: 99.1 us; the launch traced here: 98.9 us
  Pallas kernels  97 us (98%)
  local copies, waits for them, and re-layouts  1.87 us (2%)
    pallas_call x1, Pallas kernels, on_device_any(): pl.pallas_call(functools.partial(fused_kernel, ra_count, cb_count), out_s...  97 us

profile of v1, /device:TPU:0, one launch (start us, length us, event | category | flops | bytes accessed | tf_op | source)
XLA Modules:
  0.0 98.9 jit_solution(8281370838353936833)
XLA Ops:
  0.0 97.0 %fused_sublayers.1 = bf16[4,64,1024]{2,1,0:T(8,128)(2,1)} custom-call(bf16[4,64,1024]{2,1,0:T(8,128)(2,1)} %bitcast.5, f32[3,1024]{1,0:T(4,128)} %gains.1, f32[2,1024,2816]{2,1,0:T(8,128)} %gate_hbm.1, f32[2,1024,2816]{2,1,0:T(8,128)} %value_hbm.1, f32[2,2816]{1,0:T(2,128)} %gate_scale.1, f32[2,2816]{1,0:T(2,128)} %value_scale.1, f32[3,2,2816]{2,1,0:T(2,128)} %bitcast.6, ...), custom_call_target="tpu_custom_call" | custom-call | tf_op jit(solution)/shard_map/fused_sublayers/pallas_call | solution.py:610
  97.1 1.9 %copy.12 = bf16[256,1024]{1,0:T(8,128)(2,1)} copy(bf16[256,1024]{1,0:T(8,128)(2,1)} %bitcast.4) | data formatting | bytes 1048576

commit v2 on v1

--- a/solution.py
+++ b/solution.py
@@ -83,28 +83,36 @@
 CORES = 2
 LANES = 128
 GROUP = 64
-RING = 13
+RING = 12
 WIDE_SLOTS = 16
 DOWN_SLOTS = 16
 FIRST_LOADS = 6
 DOWN_LAG = 3
-BUBBLES = 3
-PAIR_SUM, GATED, PAIR_GATHER, DOWN = 2, 5, 8, 10
-Z_SUM, Z_GATHER, Z_SCALE = 6, 12, 13
+BUBBLES = 2
+PAIR_SUM, GATED, PAIR_GATHER, DOWN = 1, 5, 8, 9
+Z_SUM, Z_GATHER = 5, 12
+LAST_SUM, LAST_SQUARES, LAST_GATHER = 9, 13, 22
 
 
 def fused_kernel(
     ra_count,
     cb_count,
-    tokens,
-    gains,
+    tokens_hbm,
+    gains_hbm,
     gate_hbm,
     value_hbm,
+    gate_scale_hbm,
+    value_scale_hbm,
+    conv_gate_hbm,
+    conv_value_hbm,
+    down_hbm,
+    down_scale_hbm,
+    out_hbm,
+    gains,
     gate_scale,
     value_scale,
     conv_gate,
     conv_value,
-    down_hbm,
     down_scale,
     out,
     wide_weight,
@@ -126,6 +134,11 @@
     z_own,
     sq_send,
     sq_recv,
+    last_send,
+    last_recv,
+    block_recv,
+    small_sem,
+    out_sem,
     wide_sem,
     down_sem,
     pair_ss,
@@ -142,19 +155,21 @@
     c_rs,
     sq_ss,
     sq_rs,
+    last_ss,
+    last_rs,
+    block_ss,
+    block_rs,
 ):
     f32, bf16 = jnp.float32, jnp.bfloat16
     layers = gate_hbm.shape[0]
-    groups = tokens.shape[0]
-    rows = tokens.shape[1]
-    width = tokens.shape[2]
+    groups, _, z_block, width = tokens_hbm.shape
+    rows = ra_count * z_block
     x_count = cb_count // CORES
     chunk_cols = x_count * LANES
     chunks = gate_hbm.shape[2] // chunk_cols
     pairs = pl.cdiv(chunks, CORES)
     taps = conv_gate.shape[0]
     model_width = width * cb_count
-    z_block = rows // ra_count
     per_layer = groups * pairs
     period = per_layer + BUBBLES
     last_item = layers * period - BUBBLES
@@ -217,17 +232,34 @@
             for copy in copies(n):
                 copy.start()
 
+    barrier = pltpu.get_barrier_semaphore()
+    for axis, peers in (("cb", cb_peers), ("ra", ra_peers)):
+        for peer in peers:
+            pl.semaphore_signal(
+                barrier, inc=1, device_id={axis: peer}, device_id_type=pl.DeviceIdType.MESH
+            )
+
+    small = [
+        pltpu.make_async_copy(source, place, small_sem.at[n])
+        for n, (source, place) in enumerate(
+            (
+                (tokens_hbm, current.at[0]),
+                (gains_hbm, gains),
+                (gate_scale_hbm, gate_scale),
+                (value_scale_hbm, value_scale),
+                (conv_gate_hbm, conv_gate),
+                (conv_value_hbm, conv_value),
+                (down_scale_hbm, down_scale),
+            )
+        )
+    ]
+    for copy in small[:2]:
+        copy.start()
     for n in range(min(FIRST_LOADS, streamed)):
         for copy in wide_copies(n):
             copy.start()
-
-    barrier = pltpu.get_barrier_semaphore()
-    for axis, count, me in (("cb", cb_count, me_cb), ("ra", ra_count, me_ra)):
-        for peer in others(count, me):
-            pl.semaphore_signal(
-                barrier, inc=1, device_id={axis: peer}, device_id_type=pl.DeviceIdType.MESH
-            )
-    pl.semaphore_wait(barrier, cb_count + ra_count - 2)
+    for copy in small[2:]:
+        copy.start()
 
     def pair_copy(slot):
         return remote(
@@ -277,8 +309,10 @@
         scaled[group] = (wide * gains[pl.ds(layer, 1), :]).astype(bf16).astype(f32)
         squares = jnp.broadcast_to(jnp.sum(wide * wide, axis=1, keepdims=True), (rows, LANES))
         sq_send[event] = jnp.concatenate([squares] * (LANES // rows), axis=0).T[:8]
+
+    def send_squares(layer, group):
         for peer in cb_peers:
-            sq_copy(event, peer, me_cb).start()
+            sq_copy(layer * groups + group, peer, me_cb).start()
 
     def finish_squares(layer, group):
         event = layer * groups + group
@@ -291,9 +325,15 @@
         row = lax.rsqrt(total / model_width + epsilon)
         inverse[group] = jnp.broadcast_to(row[:1], (LANES, LANES)).T[:rows]
 
+    for copy in small[:2]:
+        copy.wait()
     for group in range(groups):
-        current[0, group] = tokens[group].reshape(ra_count, z_block, width)
         scale_rows(0, group)
+    pl.semaphore_wait(barrier, cb_count + ra_count - 2)
+    for group in range(groups):
+        send_squares(0, group)
+    for copy in small[2:]:
+        copy.wait()
 
     def when_full(pair, both, first_only):
         if chunks % CORES == 0:
@@ -314,7 +354,7 @@
         else:
             pl.when((pair < pairs - 1) | (me_core == 1))(fn)
 
-    def project(layer, group, pair, slot):
+    def project_ready(layer, group, pair, slot):
         ordinal = group * pairs + pair
         first = layer * chunks + pair * CORES
         end = (layer + 1) * chunks
@@ -337,6 +377,9 @@
                 def _(n=n):
                     for copy in wide_copies(first + n):
                         copy.wait()
+
+    def project_parts(layer, group, pair, slot):
+        first = layer * chunks + pair * CORES
 
         def product_of(chunk_at):
             return jnp.dot(
@@ -374,7 +417,11 @@
                 give(first)
                 pair_copy(slot).start()
 
-        when_full(pair, both, first_only)
+        return both, first_only
+
+    def project_done(layer, group, pair, slot):
+        first = layer * chunks + pair * CORES
+        end = (layer + 1) * chunks
 
         @pl.when(group == groups - 1)
         def _():
@@ -447,7 +494,7 @@
 
         when_owner(pair, forward)
 
-    def project_down(layer, group, pair, slot):
+    def down_ready(layer, group, pair, slot):
         first = layer * chunks + pair * CORES
         end = (layer + 1) * chunks
 
@@ -462,6 +509,9 @@
 
         when_owner(pair, lambda: hp_copy(slot, me_core).wait_send())
         when_partner(pair, lambda: hp_copy(slot, 1 - me_core).wait_recv())
+
+    def down_parts(layer, group, pair, slot):
+        first = layer * chunks + pair * CORES
 
         def add(count):
             left = jnp.concatenate([hidden[slot, n] for n in range(count * x_count)], axis=1).astype(f32)
@@ -472,7 +522,11 @@
             before = acc[...]
             acc[...] = jnp.where(pair == 0, jnp.zeros_like(before), before) + product
 
-        when_full(pair, lambda: add(CORES), lambda: add(1))
+        return lambda: add(CORES), lambda: add(1)
+
+    def down_done(layer, group, pair, slot):
+        first = layer * chunks + pair * CORES
+        end = (layer + 1) * chunks
 
         @pl.when(group == groups - 1)
         def _():
@@ -500,37 +554,82 @@
             copy.wait_recv()
             total = total + z_recv[part, peer].astype(f32)
         kept = residual_weight * current[layer, group, me_ra].astype(f32)
-        current[layer + 1, group, me_ra] = (kept + down_scale[pl.ds(layer, 1), :] * total).astype(bf16)
+        block = (kept + down_scale[pl.ds(layer, 1), :] * total).astype(bf16)
+        current[layer + 1, group, me_ra] = block
         for peer in ra_peers:
             c_copy(part, layer + 1, group, peer, me_ra).start()
-
-    def z_gather(layer, group, pair, slot):
+        return block
+
+    def last_sum(layer, group, pair, slot):
+        wide = z_sum(layer, group, pair, slot).astype(f32)
+        squares = jnp.broadcast_to(jnp.sum(wide * wide, axis=1, keepdims=True), (z_block, LANES))
+        last_send[group] = jnp.concatenate([squares] * (LANES // z_block), axis=0).T[:8]
+        for peer in cb_peers:
+            last_copy(group, peer, me_cb).start()
+
+    def last_squares(layer, group, pair, slot):
+        total = last_send[group]
+        for peer in cb_peers:
+            copy = last_copy(group, peer, peer)
+            copy.wait_send()
+            copy.wait_recv()
+            total = total + last_recv[group, peer]
+        block_recv[group, me_ra] = total
+        for peer in ra_peers:
+            block_copy(group, peer, me_ra).start()
+
+    def wait_blocks(layer, group):
         part = layer * groups + group
         for peer in ra_peers:
             c_copy(part, layer + 1, group, peer, me_ra).wait_send()
             c_copy(part, layer + 1, group, peer, peer).wait_recv()
+
+    def z_gather(layer, group, pair, slot):
+        wait_blocks(layer, group)
         scale_rows(layer + 1, group)
-
-    def z_scale(layer, group, pair, slot):
-        @pl.when(layer == layers - 1)
-        def _():
-            finish_squares(layers, group)
-            wide = current[layers, group].reshape(rows, width).astype(f32)
-            inv = jnp.concatenate([inverse[group]] * (width // LANES), axis=1)
-            out[group] = (wide * inv * gains[pl.ds(layers, 1), :]).astype(bf16)
+        send_squares(layer + 1, group)
+
+    def last_gather(layer, group, pair, slot):
+        wait_blocks(layer, group)
+        for peer in ra_peers:
+            block_copy(group, peer, me_ra).wait_send()
+            block_copy(group, peer, peer).wait_recv()
+        lane = lax.broadcasted_iota(jnp.int32, (8, LANES), 1)
+        squares = jnp.zeros((8, LANES), f32)
+        for ra_at in range(ra_count):
+            inside = (lane >= ra_at * z_block) & (lane < (ra_at + 1) * z_block)
+            squares = jnp.where(inside, block_recv[group, ra_at], squares)
+        row = lax.rsqrt(squares / model_width + epsilon)
+        inv = jnp.broadcast_to(row[:1], (LANES, LANES)).T[:rows]
+        wide = current[layers, group].reshape(rows, width).astype(f32)
+        inv = jnp.concatenate([inv] * (width // LANES), axis=1)
+        out[group] = (wide * inv * gains[pl.ds(layers, 1), :]).astype(bf16)
+        out_copy(group).start()
+
+    def out_copy(group):
+        return pltpu.make_async_copy(out.at[group], out_hbm.at[group], out_sem.at[group])
+
+    def last_copy(group, peer, source):
+        return remote(
+            last_send.at[group], last_recv.at[group, source], last_ss.at[group, peer], last_rs.at[group, source], "cb", peer
+        )
+
+    def block_copy(group, peer, source):
+        place = block_recv.at[group, source]
+        return remote(place, place, block_ss.at[group, peer], block_rs.at[group, source], "ra", peer)
 
     stages = (
-        (DOWN + Z_SCALE, True, z_scale),
-        (DOWN + Z_GATHER, True, z_gather),
-        (DOWN + Z_SUM, True, z_sum),
-        (PAIR_GATHER, False, pair_gather),
-        (GATED, False, gated),
-        (PAIR_SUM, False, pair_sum),
-        (0, False, project),
-        (DOWN, False, project_down),
+        (DOWN + LAST_GATHER, "last", last_gather),
+        (DOWN + LAST_SQUARES, "last", last_squares),
+        (DOWN + LAST_SUM, "last", last_sum),
+        (DOWN + Z_GATHER, "inner", z_gather),
+        (DOWN + Z_SUM, "inner", z_sum),
+        (PAIR_GATHER, "", pair_gather),
+        (GATED, "", gated),
     )
-
-    delays = sorted({delay for delay, _, _ in stages})
+    late_stages = ((PAIR_SUM, "", pair_sum),)
+
+    delays = sorted({delay for delay, _, _ in stages + late_stages} | {0, DOWN})
 
     def started(delay):
         layer, rest = divmod(-delay, period)
@@ -547,21 +646,55 @@
         next_layer = group == all_groups
         return jnp.where(next_layer, layer + 1, layer), jnp.where(next_layer, 0, group), pair, slot
 
+    def multiply(wide_place, down_place):
+        def valid(place):
+            return (place[0] >= 0) & (place[0] < layers) & (place[1] < groups)
+
+        def full(place):
+            return place[2] < pairs - chunks % CORES
+
+        wide_on, down_on = valid(wide_place), valid(down_place)
+        merged = wide_on & down_on & full(wide_place) & full(down_place)
+        pl.when(wide_on)(lambda: project_ready(*wide_place))
+        pl.when(down_on)(lambda: down_ready(*down_place))
+
+        @pl.when(merged)
+        def _():
+            project_parts(*wide_place)[0]()
+            down_parts(*down_place)[0]()
+
+        @pl.when(wide_on & jnp.logical_not(merged))
+        def _():
+            when_full(wide_place[2], *project_parts(*wide_place))
+
+        @pl.when(down_on & jnp.logical_not(merged))
+        def _():
+            when_full(down_place[2], *down_parts(*down_place))
+
+        pl.when(wide_on)(lambda: project_done(*wide_place))
+        pl.when(down_on)(lambda: down_done(*down_place))
+
     def step(index, places):
-        for delay, at_end, stage in stages:
+        run_stages(stages, places)
+        multiply(places[delays.index(0)], places[delays.index(DOWN)])
+        run_stages(late_stages, places)
+        return tuple(advanced(place) for place in places)
+
+    def run_stages(chosen, places):
+        for delay, ending, stage in chosen:
             place = places[delays.index(delay)]
             layer, group, pair, slot = place
             valid = (layer >= 0) & (layer < layers) & (group < groups)
-            if at_end:
-                valid = valid & (pair == pairs - 1)
+            if ending:
+                valid = valid & (pair == pairs - 1) & ((layer == layers - 1) == (ending == "last"))
 
             @pl.when(valid)
             def _(stage=stage, place=place):
                 stage(*place)
 
-        return tuple(advanced(place) for place in places)
-
-    lax.fori_loop(0, last_item + DOWN + Z_SCALE, step, tuple(started(delay) for delay in delays))
+    lax.fori_loop(0, last_item + DOWN + LAST_GATHER, step, tuple(started(delay) for delay in delays))
+    for group in range(groups):
+        out_copy(group).wait()
 
 
 def fits(ra_count, cb_count, tokens, gate_weight, conv_gate):
@@ -604,15 +737,23 @@
     chunk_cols = x_count * LANES
     pairs = pl.cdiv(units // chunk_cols, CORES)
     z_block = rows // ra_count
-    parts, events = layers * groups, (layers + 1) * groups
+    parts, events = layers * groups, layers * groups
     vmem, dma = pltpu.VMEM, pltpu.SemaphoreType.DMA
-    in_vmem, in_hbm = pl.BlockSpec(memory_space=pltpu.VMEM), pl.BlockSpec(memory_space=pl.ANY)
+    in_hbm = pl.BlockSpec(memory_space=pl.ANY)
+    taps = conv_gate.shape[1]
     result = pl.pallas_call(
         functools.partial(fused_kernel, ra_count, cb_count),
         out_shape=jax.ShapeDtypeStruct((groups, rows, width), bf16),
-        in_specs=[in_vmem, in_vmem, in_hbm, in_hbm] + [in_vmem] * 4 + [in_hbm, in_vmem],
-        out_specs=in_vmem,
+        in_specs=[in_hbm] * 10,
+        out_specs=in_hbm,
         scratch_shapes=[
+            vmem(norm_gains.shape, f32),
+            vmem(gate_scale.shape, f32),
+            vmem(value_scale.shape, f32),
+            vmem((taps, layers, units), f32),
+            vmem((taps, layers, units), f32),
+            vmem(down_scale.shape, f32),
+            vmem((groups, rows, width), bf16),
             vmem((WIDE_SLOTS, width, 2 * chunk_cols), f32),
             vmem((DOWN_SLOTS, chunk_cols, width), f32),
             vmem((layers + 1, groups, ra_count, z_block, width), bf16),
@@ -632,6 +773,11 @@
             vmem((parts, z_block, width), f32),
             vmem((events, 8, LANES), f32),
             vmem((events, cb_count, 8, LANES), f32),
+            vmem((groups, 8, LANES), f32),
+            vmem((groups, cb_count, 8, LANES), f32),
+            vmem((groups, ra_count, 8, LANES), f32),
+            dma((7,)),
+            dma((groups,)),
             dma((WIDE_SLOTS, 2)),
             dma((DOWN_SLOTS,)),
             dma((RING,)),
@@ -648,13 +794,17 @@
             dma((parts, ra_count)),
             dma((events, cb_count)),
             dma((events, cb_count)),
+            dma((groups, cb_count)),
+            dma((groups, cb_count)),
+            dma((groups, ra_count)),
+            dma((groups, ra_count)),
         ],
         compiler_params=pltpu.CompilerParams(
             collective_id=0, has_side_effects=True, vmem_limit_bytes=67043328
         ),
         name="fused_sublayers",
     )(
-        tokens.reshape(groups, rows, width),
+        tokens.reshape(groups, ra_count, z_block, width),
         norm_gains,
         gate_weight,
         value_weight,

time: 99.1 us -> 94.6 us (0.955)
  Pallas kernels: 97 us -> 92.5 us
    pallas_call x1, Pallas kernels: 97 us -> 92.5 us  [on_device_any(): pl.pallas_call(functools.partial(fused_kernel, ra_count, cb_count), out_s...]
where the time goes in v2:
time: 94.6 us; the launch traced here: 94.4 us
  Pallas kernels  92.5 us (98%)
  local copies, waits for them, and re-layouts  1.87 us (2%)
    pallas_call x1, Pallas kernels, on_device_any(): pl.pallas_call(functools.partial(fused_kernel, ra_count, cb_count), out_s...  92.5 us

profile of v2, /device:TPU:0, one launch (start us, length us, event | category | flops | bytes accessed | tf_op | source)
XLA Modules:
  0.0 94.4 jit_solution(2629877531496209883)
XLA Ops:
  0.0 92.5 %fused_sublayers.1 = bf16[4,64,1024]{2,1,0:T(8,128)(2,1)} custom-call(bf16[4,4,16,1024]{3,2,1,0:T(8,128)(2,1)} %bitcast.5, f32[3,1024]{1,0:T(4,128)} %gains_hbm.1, f32[2,1024,2816]{2,1,0:T(8,128)} %gate_hbm.1, f32[2,1024,2816]{2,1,0:T(8,128)} %value_hbm.1, f32[2,2816]{1,0:T(2,128)} %gate_scale_hbm.1, f32[2,2816]{1,0:T(2,128)} %value_scale_hbm.1, ...), custom_call_target="tpu_custom_call" | custom-call | tf_op jit(solution)/shard_map/fused_sublayers/pallas_call | solution.py:744
  92.5 1.9 %copy.12 = bf16[256,1024]{1,0:T(8,128)(2,1)} copy(bf16[256,1024]{1,0:T(8,128)(2,1)} %bitcast.4) | data formatting | bytes 1048576

commit v3 on v2

--- a/solution.py
+++ b/solution.py
@@ -194,7 +194,12 @@
             device_id_type=pl.DeviceIdType.MESH,
         )
 
-    cb_peers, ra_peers, x_peers = others(cb_count, me_cb), others(ra_count, me_ra), others(x_count, me_x)
+    def far_first(count, me):
+        low = [jnp.where(n >= me, n + 1, n) for n in range(count - 1)]
+        high = [jnp.where(count - 1 - n <= me, count - 2 - n, count - 1 - n) for n in range(count - 1)]
+        return [jnp.where(2 * me < count, up, down) for up, down in zip(high, low)]
+
+    cb_peers, ra_peers, x_peers = others(cb_count, me_cb), far_first(ra_count, me_ra), others(x_count, me_x)
 
     def cb_of(x_index):
         return x_index * CORES + me_core
@@ -327,11 +332,9 @@
 
     for copy in small[:2]:
         copy.wait()
-    for group in range(groups):
-        scale_rows(0, group)
+    scale_rows(0, 0)
     pl.semaphore_wait(barrier, cb_count + ra_count - 2)
-    for group in range(groups):
-        send_squares(0, group)
+    send_squares(0, 0)
     for copy in small[2:]:
         copy.wait()
 
@@ -358,6 +361,11 @@
         ordinal = group * pairs + pair
         first = layer * chunks + pair * CORES
         end = (layer + 1) * chunks
+
+        @pl.when((layer == 0) & (group > 0) & (pair == 0))
+        def _():
+            scale_rows(0, group)
+            send_squares(0, group)
 
         @pl.when(layer == 0)
         def _():
@@ -404,7 +412,6 @@
 
         def both():
             give(first + 1 - me_core)
-            pair_copy(slot).start()
             keep(first + me_core)
 
         def first_only():
@@ -415,7 +422,6 @@
             @pl.when(me_core == 1)
             def _():
                 give(first)
-                pair_copy(slot).start()
 
         return both, first_only
 
@@ -671,7 +677,11 @@
         def _():
             when_full(down_place[2], *down_parts(*down_place))
 
-        pl.when(wide_on)(lambda: project_done(*wide_place))
+        @pl.when(wide_on)
+        def _():
+            when_partner(wide_place[2], lambda: pair_copy(wide_place[3]).start())
+            project_done(*wide_place)
+
         pl.when(down_on)(lambda: down_done(*down_place))
 
     def step(index, places):

time: 94.6 us -> 91.7 us (0.969)
  Pallas kernels: 92.5 us -> 89.7 us
    pallas_call x1, Pallas kernels: 92.5 us -> 89.7 us  [on_device_any(): pl.pallas_call(functools.partial(fused_kernel, ra_count, cb_count), out_s...]
where the time goes in v3:
time: 91.7 us; the launch traced here: 91.5 us
  Pallas kernels  89.7 us (98%)
  local copies, waits for them, and re-layouts  1.87 us (2%)
    pallas_call x1, Pallas kernels, on_device_any(): pl.pallas_call(functools.partial(fused_kernel, ra_count, cb_count), out_s...  89.7 us
    unnamed x1, local copies, waits for them, and re-layouts  1.87 us

profile of v3, /device:TPU:0, one launch (start us, length us, event | category | flops | bytes accessed | tf_op | source)
XLA Modules:
  0.0 91.5 jit_solution(10824223576891815195)
XLA Ops:
  0.0 89.7 %fused_sublayers.1 = bf16[4,64,1024]{2,1,0:T(8,128)(2,1)} custom-call(bf16[4,4,16,1024]{3,2,1,0:T(8,128)(2,1)} %bitcast.5, f32[3,1024]{1,0:T(4,128)} %gains_hbm.1, f32[2,1024,2816]{2,1,0:T(8,128)} %gate_hbm.1, f32[2,1024,2816]{2,1,0:T(8,128)} %value_hbm.1, f32[2,2816]{1,0:T(2,128)} %gate_scale_hbm.1, f32[2,2816]{1,0:T(2,128)} %value_scale_hbm.1, ...), custom_call_target="tpu_custom_call" | custom-call | tf_op jit(solution)/shard_map/fused_sublayers/pallas_call | solution.py:754
  89.7 1.9 %copy.12 = bf16[256,1024]{1,0:T(8,128)(2,1)} copy(bf16[256,1024]{1,0:T(8,128)(2,1)} %bitcast.4) | data formatting | bytes 1048576
